TPU v7x, 32 devices: a whole 2x2x4 slice. The times are simulated.
32 devices in a mesh: fs: 8 (over z, y), tp: 4 (over x, core).
Axes of the slice: x: 2, y: 2, z: 4, core: 2. Of those that a mesh axis runs over, the one named last changes fastest.
Arguments:
- tokens: bfloat16 [3072, 2048], P('tp'), may hold values from -6 to 6
- norm_gain: float32 [2048], P('fs'), may hold values from 0.1 to 1.9
- gate_weight: float32 [4, 2048, 8192], P(None, 'fs', 'tp'), may hold values from -0.125 to 0.125
- up_weight: float32 [4, 2048, 8192], P(None, 'fs', 'tp'), may hold values from -0.125 to 0.125
- down_weight: float32 [4, 8192, 2048], P(None, 'fs', 'tp'), may hold values from -0.0625 to 0.0625
- routes: int32 [3072, 2], P('tp'), may hold values from 0 to 3, all different within a row; in each aligned block of 768 rows (0 to 767, 768 to 1535, ...) at most 480 rows name the same one
- route_logit: float32 [3072, 2], P('tp'), may hold values from -6 to 6
Outputs:
- gate_out: bfloat16 [4, 2048, 8192], P(None, None, 'fs')
- up_out: bfloat16 [4, 2048, 8192], P(None, None, 'fs')
- down_out: bfloat16 [4, 8192, 2048], P(None, 'fs')
- mixed: bfloat16 [3072, 2048], P(('tp', 'fs'))
Inputs may be any that keep to these rules, and one draw needn't show every extreme that they name: `routes`: the two experts of a token differ. In each aligned block of 768 tokens (the tokens of one request group) every expert is named by at most 480 tokens, a bound that some block reaches.
All inputs are finite; a program needn't handle non-finite values.
Results may differ from a plain program's by a relative error of at most 0.0082.
Values may be sent and summed in bfloat16 or wider, within the bound.
No kernel may reach another device: no remote copies, remote signals or barrier semaphores. Data moves between devices by JAX's collectives and lax.ppermute only.
A program may use at most 192 MiB of HBM per device.

v0:
```python
import jax
import jax.numpy as jnp
from jax import lax
from jax.sharding import PartitionSpec as P

EPS = 0.5


def shards(tokens, norm_gain, gate_weight, up_weight, down_weight, routes, route_logit):
    gain_col = norm_gain[None, :, None]
    gate_part = (gate_weight * gain_col).astype(jnp.bfloat16)
    up_part = (up_weight * gain_col).astype(jnp.bfloat16)
    down_part = down_weight.astype(jnp.bfloat16)
    gate_one, up_one = (
        lax.all_to_all(gate_part, "tp", split_axis=0, concat_axis=2, tiled=True),
        lax.all_to_all(up_part, "tp", split_axis=0, concat_axis=2, tiled=True),
    )
    gate_mine, up_mine = (
        lax.all_to_all(gate_one, "fs", split_axis=2, concat_axis=1, tiled=True),
        lax.all_to_all(up_one, "fs", split_axis=2, concat_axis=1, tiled=True),
    )
    gate_out, up_out = (
        lax.all_gather(gate_mine, "tp", axis=0, tiled=True),
        lax.all_gather(up_mine, "tp", axis=0, tiled=True),
    )
    down_out = lax.all_gather(down_part, "tp", axis=2, tiled=True)
    total_rows = tokens.shape[0]
    width = tokens.shape[1]
    experts = gate_out.shape[0]
    capacity = total_rows * 5 // 8
    floats = tokens.astype(jnp.float32)
    normed = (floats * lax.rsqrt(jnp.mean(floats * floats, axis=1, keepdims=True) + EPS)).astype(
        jnp.bfloat16
    )
    first_share = jax.nn.sigmoid(route_logit[:, 0] - route_logit[:, 1])
    shares = jnp.stack([first_share, 1.0 - first_share], axis=1)
    chosen = (routes[:, :, None] == jnp.arange(experts, dtype=jnp.int32)[None, None, :]).astype(
        jnp.int32
    )
    counts = jnp.sum(chosen, axis=1)
    before = jnp.cumsum(counts, axis=0) - counts
    slot_index = jnp.sum(chosen * before[:, None, :], axis=2)
    flat_slot = routes * capacity + slot_index
    row_ids = jnp.repeat(jnp.arange(total_rows, dtype=jnp.int32), 2)
    table = (
        jnp.full((experts * capacity,), total_rows, jnp.int32)
        .at[flat_slot.reshape(-1)]
        .set(row_ids)
    )
    gathered = jnp.take(normed, table, axis=0, mode="fill", fill_value=0).reshape(
        experts, capacity, width
    )
    gate_val = jnp.einsum("ecd,edf->ecf", gathered, gate_out, preferred_element_type=jnp.float32)
    up_val = jnp.einsum("ecd,edf->ecf", gathered, up_out, preferred_element_type=jnp.float32)
    hidden = (jax.nn.silu(gate_val) * up_val).astype(jnp.bfloat16)
    results = jnp.einsum("ecf,efd->ecd", hidden, down_out, preferred_element_type=jnp.float32)
    flat_rows = results.reshape(experts * capacity, width)
    first_rows = jnp.take(flat_rows, flat_slot[:, 0], axis=0)
    second_rows = jnp.take(flat_rows, flat_slot[:, 1], axis=0)
    mixed = lax.psum_scatter(
        shares[:, 0:1] * first_rows + shares[:, 1:2] * second_rows,
        "fs",
        scatter_dimension=0,
        tiled=True,
    )
    return (gate_out, up_out, down_out, mixed.astype(jnp.bfloat16))


def solution(mesh):
    return jax.shard_map(
        shards,
        mesh=mesh,
        in_specs=(
            P("tp", None),
            P("fs"),
            P(None, "fs", "tp"),
            P(None, "fs", "tp"),
            P(None, "fs", "tp"),
            P("tp", None),
            P("tp", None),
        ),
        out_specs=(
            P(None, None, "fs"),
            P(None, None, "fs"),
            P(None, "fs", None),
            P(("tp", "fs"), None),
        ),
        check_vma=False,
    )
```

profile of v0, /device:TPU:0, one launch (start us, length us, event | category | flops | bytes accessed | tf_op | source)
XLA Modules:
  0.0 959.0 jit_solution(9687158230475078291)
XLA Ops:
  7.2 0.0 all-gather.6.cloned.1.call-start
  7.2 8.7 copy.43
  15.9 0.0 copy-start.3
  15.9 8.7 copy.46
  24.6 0.0 copy-done.3
  24.6 10.7 %multiply_convert_fusion = (bf16[4,256,2048]{1,2,0:T(8,128)(2,1)}, bf16[4,256,2048]{1,2,0:T(8,128)(2,1)}) fusion(f32[4,256,2048]{1,2,0:T(8,128)} %copy.46, f32[256]{0:T(256)S(1)} %copy-done.3, f32[4,256,2048]{1,2,0:T(8,128)} %copy.43), kind=kLoop, calls=%fused_computation.4 | loop fusion | flops 8388608 | bytes 25166848 | tf_op jit(solution)/shard_map/convert_element_type | solution.py:12
  35.3 52.6 %all_to_all.72 = bf16[4,256,2048]{1,2,0:T(8,128)(2,1)S(1)} all-to-all(bf16[4,256,2048]{1,2,0:T(8,128)(2,1)} %get-tuple-element.9), channel_id=1, replica_groups=mesh['fs'=8,'tp'=4] {'tp'}, dimensions={0} | all-to-all | bytes 8388608 | tf_op jit(solution)/shard_map/all_to_all | solution.py:16
  87.9 49.3 %copy.56 = bf16[1,256,8192]{1,0,2:T(2,128)(2,1)} copy(bf16[1,256,8192]{1,2,0:T(8,128)(2,1)S(1)} %bitcast.49) | data formatting | bytes 8388608 | tf_op jit(solution)/shard_map/all_to_all | solution.py:16
  137.2 0.5 broadcast.78
  137.7 43.5 %reduce.13 = bf16[8192,256]{1,0:T(8,128)(2,1)} reduce(bf16[8192,1,256]{2,1,0:T(2,128)(2,1)} %bitcast.45, bf16[]{:T(256)} %broadcast.78), dimensions={1}, to_apply=%bitcast.40.reduce_sub_computation | reduce | bytes 8388610
  181.2 6.9 reshape.137
  188.2 99.8 %all_to_all.73 = bf16[8,2,131072]{2,1,0:T(2,128)(2,1)} all-to-all(bf16[8,2,131072]{2,1,0:T(2,128)(2,1)} %reshape.137), channel_id=1, replica_groups=mesh['fs'=8,'tp'=4] {'fs'}, dimensions={0} | all-to-all | bytes 8388608 | tf_op jit(solution)/shard_map/all_to_all | solution.py:20
  288.0 8.7 reshape.138
  296.7 6.1 copy.51
  302.8 6.4 copy.48
  309.3 0.0 all-gather.6.cloned.1.call-update
  309.3 0.0 all-gather.8.cloned.1.call-start
  309.3 6.0 convert_element_type.26
  315.4 0.0 all-gather.8.cloned.1.call-update
  315.4 0.0 all-gather.4.cloned.1.call-start
  315.4 97.4 %all_to_all.74 = bf16[4,256,2048]{1,2,0:T(8,128)(2,1)S(1)} all-to-all(bf16[4,256,2048]{1,2,0:T(8,128)(2,1)} %get-tuple-element.10), channel_id=1, replica_groups=mesh['fs'=8,'tp'=4] {'tp'}, dimensions={0} | all-to-all | bytes 8388608 | tf_op jit(solution)/shard_map/all_to_all | solution.py:15
  412.8 49.3 %copy.57 = bf16[1,256,8192]{1,0,2:T(2,128)(2,1)} copy(bf16[1,256,8192]{1,2,0:T(8,128)(2,1)S(1)} %bitcast.51) | data formatting | bytes 8388608 | tf_op jit(solution)/shard_map/all_to_all | solution.py:15
  462.2 43.5 %reduce.12 = bf16[8192,256]{1,0:T(8,128)(2,1)} reduce(bf16[8192,1,256]{2,1,0:T(2,128)(2,1)} %bitcast.46, bf16[]{:T(256)} %broadcast.78), dimensions={1}, to_apply=%bitcast.41.reduce_sub_computation | reduce | bytes 8388610
  505.7 7.0 reshape.135
  512.7 97.7 %all_to_all.75 = bf16[8,2,131072]{2,1,0:T(2,128)(2,1)} all-to-all(bf16[8,2,131072]{2,1,0:T(2,128)(2,1)} %reshape.135), channel_id=1, replica_groups=mesh['fs'=8,'tp'=4] {'fs'}, dimensions={0} | all-to-all | bytes 8388608 | tf_op jit(solution)/shard_map/all_to_all | solution.py:19
  610.4 8.7 reshape.136
  619.1 6.1 copy.50
  625.2 0.0 copy-start.1
  625.2 6.6 copy.45
  631.8 0.0 all-gather.4.cloned.1.call-update
  631.8 0.0 reduce-scatter.2.cloned.1.call-start
  631.9 0.0 copy-done.1
  631.9 1.1 reduce-window.6
  633.1 0.2 slice_reduce_fusion
  633.3 0.2 reduce-window.9
  633.5 0.1 add_bitcast_fusion
  633.6 0.2 copy.49
  633.8 0.3 reshape.85
  634.1 0.8 reshape.116
  634.9 6.3 scatter_custom_fusion
  641.3 0.1 broadcast_in_dim.37
  641.4 0.0 copy-done
  641.4 0.7 fusion.2
  642.1 2.8 fusion.3
  644.9 0.0 copy-start.2
  644.9 8.9 gather_fusion
  653.9 0.0 copy-done.2
  653.9 0.0 all-gather.6.cloned.1.call-done
  654.0 16.3 %fusion = f32[4,480,1024]{2,1,0:T(8,128)} fusion(bf16[4,2048,1024]{2,1,0:T(8,128)(2,1)} %all-gather.6.cloned.1.call-done, bf16[4,480,2048]{2,1,0:T(8,128)(2,1)} %bitcast.57, pred[4,480]{1,0:T(4,128)(4,1)S(1)} %broadcast_in_dim.37), kind=kOutput, calls=%fused_computation.10 | convolution fusion | flops 8056995840 | bytes 32507776 | tf_op jit(solution)/shard_map/ecd,edf->ecf/dot_general | solution.py:54
  670.2 65.7 %all-gather.4.cloned.1.call-done = bf16[4,2048,1024]{2,1,0:T(8,128)(2,1)} async-done(((bf16[1,2048,1024]{2,1,0:T(8,128)(2,1)}), bf16[4,2048,1024]{2,1,0:T(8,128)(2,1)}) %all-gather.4.cloned.1.call-update) | async-done | bytes 16777232 | tf_op jit(solution)/shard_map/all_gather | solution.py:23
  735.9 27.2 %fusion.7 = f32[4,480,2048]{2,1,0:T(8,128)} fusion(bf16[4,1024,2048]{2,1,0:T(8,128)(2,1)} %all-gather.8.cloned.1.call-done, f32[4,480,1024]{2,1,0:T(8,128)} %fusion, bf16[4,2048,1024]{2,1,0:T(8,128)(2,1)} %all-gather.4.cloned.1.call-done, bf16[4,480,2048]{2,1,0:T(8,128)(2,1)} %bitcast.58, pred[4,480]{1,0:T(4,128)(4,1)S(1)} %broadcast_in_dim.37), kind=kOutput, calls=%fused_computation.19 | convolution fusion | flops 16121856000 | bytes 65013632 | tf_op jit(solution)/shard_map/ecf,efd->ecd/dot_general | solution.py:56
  763.1 12.7 %gather_fusion.1 = f32[768,2048]{1,0:T(8,128)} fusion(f32[1920,2048]{1,0:T(8,128)} %bitcast.43, s32[1024]{0:T(1024)S(1)} %pad_clamp_fusion.2), kind=kCustom, calls=%fused_computation.clone | custom fusion | bytes 12585984 | tf_op jit(solution)/shard_map/jit(_take)/gather | solution.py:58
  775.8 12.7 %gather_fusion.2 = f32[768,2048]{1,0:T(8,128)} fusion(f32[1920,2048]{1,0:T(8,128)} %bitcast.44, s32[1024]{0:T(1024)S(1)} %pad_clamp_fusion.1), kind=kCustom, calls=%fused_computation.1.clone | custom fusion | bytes 12585984 | tf_op jit(solution)/shard_map/jit(_take)/gather | solution.py:59
  788.5 7.2 fusion.4
  795.7 0.0 reduce-scatter.2.cloned.1.call-update
  795.7 118.2 %reduce-scatter.2.cloned.1.call-done = f32[96,2048]{1,0:T(8,128)} async-done(((f32[768,2048]{1,0:T(8,128)}), f32[96,2048]{1,0:T(8,128)}) %reduce-scatter.2.cloned.1.call-update) | async-done | bytes 786448 | tf_op jit(solution)/shard_map/reduce_scatter | solution.py:60
  913.9 1.9 convert_element_type.31
  915.8 15.2 %copy.61 = bf16[4,2048,1024]{2,1,0:T(8,128)(2,1)} copy(bf16[4,2048,1024]{2,1,0:T(8,128)(2,1)} %all-gather.4.cloned.1.call-done) | data formatting | bytes 33554432
  931.1 15.2 %copy.62 = bf16[4,2048,1024]{2,1,0:T(8,128)(2,1)} copy(bf16[4,2048,1024]{2,1,0:T(8,128)(2,1)} %all-gather.6.cloned.1.call-done) | data formatting | bytes 33554432
  946.3 0.0 slice-done
  946.3 0.0 slice-done.1
  946.3 0.0 slice-done.2
  946.3 0.0 slice-done.3
  946.3 6.2 copy.63
  (24 shorter events, 0.3 us)
Async XLA Ops:
  7.2 646.8 %all-gather.6.cloned.1.call-start = ((), (), s32[]{:S(2)}) async-start(), calls=%async_computation.6 | async-start | bytes 20971520 | tf_op jit(solution)/shard_map/all_gather | solution.py:24
  15.9 8.7 copy-start.3
  309.3 360.9 %all-gather.8.cloned.1.call-start = ((), (), s32[]{:S(2)}) async-start(), calls=%async_computation.7 | async-start | bytes 20971520 | tf_op jit(solution)/shard_map/all_gather | solution.py:26
  315.4 420.5 %all-gather.4.cloned.1.call-start = ((), (), s32[]{:S(2)}) async-start(), calls=%async_computation.5 | async-start | bytes 20971520 | tf_op jit(solution)/shard_map/all_gather | solution.py:23
  625.2 6.7 copy-start.1
  625.2 16.2 %copy-start = (bf16[768,2048]{1,0:T(8,128)(2,1)S(1)}, bf16[768,2048]{1,0:T(8,128)(2,1)}, u32[]{:S(2)}) copy-start(bf16[768,2048]{1,0:T(8,128)(2,1)} %param.9) | copy-start | bytes 9437188
  631.8 282.1 %reduce-scatter.2.cloned.1.call-start = ((), (), s32[]{:S(2)}) async-start(), calls=%async_computation.8 | async-start | bytes 7077888 | tf_op jit(solution)/shard_map/reduce_scatter | solution.py:60
  644.9 8.9 copy-start.2
  915.8 30.5 %slice-start = ((s8[16777216]{0:T(1024)(128)(4,1)}), s8[4194304]{0:T(1024)(128)(4,1)S(1)}, s32[]{:S(2)}) async-start(s8[16777216]{0:T(1024)(128)(4,1)} %bitcast.53), calls=%async_computation.9 | async-start | bytes 8388608
  915.8 30.5 %slice-start.1 = ((s8[16777216]{0:T(1024)(128)(4,1)}), s8[4194304]{0:T(1024)(128)(4,1)S(1)}, s32[]{:S(2)}) async-start(s8[16777216]{0:T(1024)(128)(4,1)} %bitcast.53), calls=%async_computation.10 | async-start | bytes 8388608
  931.1 15.2 %slice-start.2 = ((s8[16777216]{0:T(1024)(128)(4,1)}), s8[4194304]{0:T(1024)(128)(4,1)S(1)}, s32[]{:S(2)}) async-start(s8[16777216]{0:T(1024)(128)(4,1)} %bitcast.53), calls=%async_computation.11 | async-start | bytes 8388608
  931.1 15.2 %slice-start.3 = ((s8[16777216]{0:T(1024)(128)(4,1)}), s8[4194304]{0:T(1024)(128)(4,1)S(1)}, s32[]{:S(2)}) async-start(s8[16777216]{0:T(1024)(128)(4,1)} %bitcast.53), calls=%async_computation.12 | async-start | bytes 8388608
Sparse Core Ops, SparseCore 0:
  309.4 148.9 all-gather.5
  460.0 104.8 all-gather.7
  631.9 103.9 all-gather.3
  795.8 118.0 reduce-scatter.1
where the time goes:
time: 961 us; the launch traced here: 959 us
  blocking collectives  347 us (36%)
  local copies, waits for them, and re-layouts  252 us (26%)
  waiting for transfers between devices  184 us (19%)
  other arithmetic  118 us (12%)
  matrix products  43.5 us (5%)
  between operations  14 us (1%)
    reduce_scatter x1, waiting for transfers between devices, shards(): lax.psum_scatter(shares[:, 0:1] * first_rows + shares[:, 1:2] * second_ro...  118 us
    all_to_all x1, blocking collectives, shards(): lax.all_to_all(up_one, 'fs', split_axis=2, concat_axis=1, tiled=True)  99.8 us
    unnamed x28, local copies, waits for them, and re-layouts  98.2 us
    all_to_all x1, blocking collectives, shards(): lax.all_to_all(gate_one, 'fs', split_axis=2, concat_axis=1, tiled=True)  97.7 us
    all_to_all x1, blocking collectives, shards(): lax.all_to_all(gate_part, 'tp', split_axis=0, concat_axis=2, tiled=True)  97.4 us
    unnamed x4, other arithmetic  87.2 us
    all_gather x1, waiting for transfers between devices, shards(): lax.all_gather(gate_mine, 'tp', axis=0, tiled=True)  65.7 us
    all_to_all x1, blocking collectives, shards(): lax.all_to_all(up_part, 'tp', split_axis=0, concat_axis=2, tiled=True)  52.6 us
  transfers between devices with their start and end apart: 4, of which 2 were waited for; matrix products, arithmetic and copies ran while one was open for 17% of the time, Pallas kernels for 0%

commit v1 on v0

--- a/solution.py
+++ b/solution.py
@@ -4,6 +4,29 @@
 from jax.sharding import PartitionSpec as P
 
 EPS = 0.5
+
+
+def cut_along(value, dim, size):
+    lengths = value.shape
+    tiles = value.reshape(*lengths[:dim], size, lengths[dim] // size, *lengths[dim + 1 :])
+    return jnp.moveaxis(tiles, dim, 0)
+
+
+def laid_out(parts, dim):
+    shape = list(parts.shape[1:])
+    shape[dim] *= parts.shape[0]
+    return jnp.moveaxis(parts, 0, dim).reshape(shape)
+
+
+def swapped_with_each(x, axis, split_dim, concat_dim):
+    size, position = (lax.axis_size(axis), lax.axis_index(axis))
+    blocks = cut_along(x, split_dim, size)
+    outs = [blocks[position]]
+    for hop in range(1, size):
+        sent = blocks[position ^ hop]
+        outs.append(lax.ppermute(sent, axis, [(i, i ^ hop) for i in range(size)]))
+    blocks = jnp.stack(outs)[position ^ jnp.arange(size)]
+    return laid_out(blocks, concat_dim)
 
 
 def shards(tokens, norm_gain, gate_weight, up_weight, down_weight, routes, route_logit):
@@ -13,7 +36,7 @@
     down_part = down_weight.astype(jnp.bfloat16)
     gate_one, up_one = (
         lax.all_to_all(gate_part, "tp", split_axis=0, concat_axis=2, tiled=True),
-        lax.all_to_all(up_part, "tp", split_axis=0, concat_axis=2, tiled=True),
+        swapped_with_each(up_part, "tp", 0, 2),
     )
     gate_mine, up_mine = (
         lax.all_to_all(gate_one, "fs", split_axis=2, concat_axis=1, tiled=True),

time: 961 us -> 926 us (0.964)
  blocking collectives: 347 us -> 295 us
  waiting for transfers between devices: 184 us -> 230 us
  local copies, waits for them, and re-layouts: 252 us -> 219 us
    all_to_all x1 -> x0, blocking collectives: 52.6 us -> none  [shards(): lax.all_to_all(up_part, 'tp', split_axis=0, concat_axis=2, tiled=True)]
    all_to_all x1 -> x0, local copies, waits for them, and re-layouts: 49.3 us -> none  [shards(): lax.all_to_all(up_part, 'tp', split_axis=0, concat_axis=2, tiled=True)]
    ppermute x0 -> x3, waiting for transfers between devices: none -> 45.9 us  [swapped_with_each(): outs.append(lax.ppermute(sent, axis, [(i, i ^ hop) for i in range(size)]))]
  transfers between devices with their start and end apart: 4 -> 7, of which waited for: 2 -> 4; matrix products, arithmetic and copies ran while one was open for 17% -> 18% of each run, Pallas kernels for 0% -> 0%
where the time goes in v1:
time: 926 us; the launch traced here: 924 us
  blocking collectives  295 us (32%)
  waiting for transfers between devices  230 us (25%)
  local copies, waits for them, and re-layouts  219 us (24%)
  other arithmetic  120 us (13%)
  matrix products  43.5 us (5%)
  between operations  14 us (2%)
    reduce_scatter x1, waiting for transfers between devices, shards(): lax.psum_scatter(shares[:, 0:1] * first_rows + shares[:, 1:2] * second_ro...  118 us
    all_to_all x1, blocking collectives, shards(): lax.all_to_all(up_one, 'fs', split_axis=2, concat_axis=1, tiled=True)  99.6 us
    unnamed x28, local copies, waits for them, and re-layouts  98.1 us
    all_to_all x1, blocking collectives, shards(): lax.all_to_all(gate_one, 'fs', split_axis=2, concat_axis=1, tiled=True)  97.8 us
    all_to_all x1, blocking collectives, shards(): lax.all_to_all(gate_part, 'tp', split_axis=0, concat_axis=2, tiled=True)  97.2 us
    unnamed x4, other arithmetic  87.2 us
    all_gather x1, waiting for transfers between devices, shards(): lax.all_gather(gate_mine, 'tp', axis=0, tiled=True)  65.7 us
    all_to_all x1, local copies, waits for them, and re-layouts, shards(): lax.all_to_all(gate_part, 'tp', split_axis=0, concat_axis=2, tiled=True)  49.3 us
  transfers between devices with their start and end apart: 7, of which 4 were waited for; matrix products, arithmetic and copies ran while one was open for 18% of the time, Pallas kernels for 0%

profile of v1, /device:TPU:0, one launch (start us, length us, event | category | flops | bytes accessed | tf_op | source)
XLA Modules:
  0.0 924.2 jit_solution(3058394377603839443)
XLA Ops:
  7.2 0.0 all-gather.6.cloned.1.call-start
  7.2 8.7 copy.43
  15.9 8.7 copy.46
  24.6 0.0 copy-done.3
  24.6 10.7 %multiply_convert_fusion = (bf16[4,256,2048]{1,2,0:T(8,128)(2,1)}, bf16[4,256,2048]{1,2,0:T(8,128)(2,1)}) fusion(f32[4,256,2048]{1,2,0:T(8,128)} %copy.46, f32[256]{0:T(256)S(1)} %copy-done.3, f32[4,256,2048]{1,2,0:T(8,128)} %copy.43), kind=kLoop, calls=%fused_computation.5 | loop fusion | flops 8388608 | bytes 25166848 | tf_op jit(solution)/shard_map/convert_element_type | solution.py:35
  35.3 2.4 dynamic-slice_bitcast_fusion
  37.8 0.6 collective-permute-start
  38.3 2.6 collective-permute-start.1
  40.9 0.0 collective-permute-start.2
  40.9 0.0 collective-permute-done
  40.9 23.9 %collective-permute-done.1 = bf16[1,256,2048]{1,2,0:T(8,128)(2,1)S(1)} collective-permute-done((bf16[1,256,2048]{1,2,0:T(8,128)(2,1)S(1)}, bf16[1,256,2048]{1,2,0:T(8,128)(2,1)S(1)}, u32[]{:S(2)}, u32[]{:S(2)}) %collective-permute-start.1) | collective-permute-done | bytes 1048608 | tf_op jit(solution)/shard_map/ppermute | solution.py:27
  64.9 21.9 %collective-permute-done.2 = bf16[1,256,2048]{1,2,0:T(8,128)(2,1)S(1)} collective-permute-done((bf16[1,256,2048]{1,2,0:T(8,128)(2,1)S(1)}, bf16[1,256,2048]{1,2,0:T(8,128)(2,1)S(1)}, u32[]{:S(2)}, u32[]{:S(2)}) %collective-permute-start.2) | collective-permute-done | bytes 1048608 | tf_op jit(solution)/shard_map/ppermute | solution.py:27
  86.8 2.3 maximum_bitcast_fusion
  89.1 5.0 gather_fusion
  94.1 8.6 copy.56
  102.7 0.5 broadcast.113
  103.2 43.5 %reduce.13 = bf16[8192,256]{1,0:T(8,128)(2,1)} reduce(bf16[8192,1,256]{2,1,0:T(2,128)(2,1)} %bitcast.54, bf16[]{:T(256)} %broadcast.113), dimensions={1}, to_apply=%bitcast.49.reduce_sub_computation | reduce | bytes 8388610
  146.8 6.9 reshape.175
  153.7 99.6 %all_to_all.54 = bf16[8,2,131072]{2,1,0:T(2,128)(2,1)} all-to-all(bf16[8,2,131072]{2,1,0:T(2,128)(2,1)} %reshape.175), channel_id=1, replica_groups=mesh['fs'=8,'tp'=4] {'fs'}, dimensions={0} | all-to-all | bytes 8388608 | tf_op jit(solution)/shard_map/all_to_all | solution.py:43
  253.3 8.7 reshape.176
  262.0 6.1 copy.51
  268.1 6.4 copy.48
  274.5 0.0 all-gather.6.cloned.1.call-update
  274.6 0.0 all-gather.8.cloned.1.call-start
  274.6 6.0 convert_element_type.26
  280.7 0.0 all-gather.8.cloned.1.call-update
  280.7 0.0 all-gather.4.cloned.1.call-start
  280.7 97.2 %all_to_all.55 = bf16[4,256,2048]{1,2,0:T(8,128)(2,1)S(1)} all-to-all(bf16[4,256,2048]{1,2,0:T(8,128)(2,1)} %get-tuple-element.14), channel_id=1, replica_groups=mesh['fs'=8,'tp'=4] {'tp'}, dimensions={0} | all-to-all | bytes 8388608 | tf_op jit(solution)/shard_map/all_to_all | solution.py:38
  377.9 49.3 %copy.57 = bf16[1,256,8192]{1,0,2:T(2,128)(2,1)} copy(bf16[1,256,8192]{1,2,0:T(8,128)(2,1)S(1)} %bitcast.60) | data formatting | bytes 8388608 | tf_op jit(solution)/shard_map/all_to_all | solution.py:38
  427.3 43.5 %reduce.12 = bf16[8192,256]{1,0:T(8,128)(2,1)} reduce(bf16[8192,1,256]{2,1,0:T(2,128)(2,1)} %bitcast.55, bf16[]{:T(256)} %broadcast.113), dimensions={1}, to_apply=%bitcast.50.reduce_sub_computation | reduce | bytes 8388610
  470.8 6.9 reshape.173
  477.8 97.8 %all_to_all.56 = bf16[8,2,131072]{2,1,0:T(2,128)(2,1)} all-to-all(bf16[8,2,131072]{2,1,0:T(2,128)(2,1)} %reshape.173), channel_id=1, replica_groups=mesh['fs'=8,'tp'=4] {'fs'}, dimensions={0} | all-to-all | bytes 8388608 | tf_op jit(solution)/shard_map/all_to_all | solution.py:42
  575.6 8.7 reshape.174
  584.3 6.1 copy.50
  590.4 6.6 copy.45
  597.0 0.0 all-gather.4.cloned.1.call-update
  597.0 0.0 reduce-scatter.2.cloned.1.call-start
  597.1 1.1 reduce-window.6
  598.3 0.2 slice_reduce_fusion
  598.5 0.2 reduce-window.9
  598.7 0.1 add_bitcast_fusion
  598.8 0.2 copy.49
  599.0 0.2 reshape.113
  599.3 0.8 reshape.154
  600.1 6.3 scatter_custom_fusion
  606.5 0.1 broadcast_in_dim.38
  606.6 0.7 fusion.2
  607.3 2.8 fusion.3
  610.1 0.0 copy-start.2
  610.1 8.9 gather_fusion.1
  619.1 0.0 all-gather.6.cloned.1.call-done
  619.2 16.3 %fusion = f32[4,480,1024]{2,1,0:T(8,128)} fusion(bf16[4,2048,1024]{2,1,0:T(8,128)(2,1)} %all-gather.6.cloned.1.call-done, bf16[4,480,2048]{2,1,0:T(8,128)(2,1)} %bitcast.66, pred[4,480]{1,0:T(4,128)(4,1)S(1)} %broadcast_in_dim.38), kind=kOutput, calls=%fused_computation.11 | convolution fusion | flops 8056995840 | bytes 32507776 | tf_op jit(solution)/shard_map/ecd,edf->ecf/dot_general | solution.py:77
  635.5 65.7 %all-gather.4.cloned.1.call-done = bf16[4,2048,1024]{2,1,0:T(8,128)(2,1)} async-done(((bf16[1,2048,1024]{2,1,0:T(8,128)(2,1)}), bf16[4,2048,1024]{2,1,0:T(8,128)(2,1)}) %all-gather.4.cloned.1.call-update) | async-done | bytes 16777232 | tf_op jit(solution)/shard_map/all_gather | solution.py:46
  701.2 27.2 %fusion.7 = f32[4,480,2048]{2,1,0:T(8,128)} fusion(bf16[4,1024,2048]{2,1,0:T(8,128)(2,1)} %all-gather.8.cloned.1.call-done, f32[4,480,1024]{2,1,0:T(8,128)} %fusion, bf16[4,2048,1024]{2,1,0:T(8,128)(2,1)} %all-gather.4.cloned.1.call-done, bf16[4,480,2048]{2,1,0:T(8,128)(2,1)} %bitcast.67, pred[4,480]{1,0:T(4,128)(4,1)S(1)} %broadcast_in_dim.38), kind=kOutput, calls=%fused_computation.21 | convolution fusion | flops 16121856000 | bytes 65013632 | tf_op jit(solution)/shard_map/ecf,efd->ecd/dot_general | solution.py:79
  728.4 12.7 %gather_fusion.2 = f32[768,2048]{1,0:T(8,128)} fusion(f32[1920,2048]{1,0:T(8,128)} %bitcast.52, s32[1024]{0:T(1024)S(1)} %pad_clamp_fusion.2), kind=kCustom, calls=%fused_computation.clone | custom fusion | bytes 12585984 | tf_op jit(solution)/shard_map/jit(_take)/gather | solution.py:81
  741.1 12.7 %gather_fusion.3 = f32[768,2048]{1,0:T(8,128)} fusion(f32[1920,2048]{1,0:T(8,128)} %bitcast.53, s32[1024]{0:T(1024)S(1)} %pad_clamp_fusion.1), kind=kCustom, calls=%fused_computation.1.clone | custom fusion | bytes 12585984 | tf_op jit(solution)/shard_map/jit(_take)/gather | solution.py:82
  753.7 7.2 fusion.4
  761.0 0.0 reduce-scatter.2.cloned.1.call-update
  761.0 118.1 %reduce-scatter.2.cloned.1.call-done = f32[96,2048]{1,0:T(8,128)} async-done(((f32[768,2048]{1,0:T(8,128)}), f32[96,2048]{1,0:T(8,128)}) %reduce-scatter.2.cloned.1.call-update) | async-done | bytes 786448 | tf_op jit(solution)/shard_map/reduce_scatter | solution.py:83
  879.1 1.9 convert_element_type.31
  881.1 15.2 %copy.61 = bf16[4,2048,1024]{2,1,0:T(8,128)(2,1)} copy(bf16[4,2048,1024]{2,1,0:T(8,128)(2,1)} %all-gather.4.cloned.1.call-done) | data formatting | bytes 33554432
  896.3 15.2 %copy.62 = bf16[4,2048,1024]{2,1,0:T(8,128)(2,1)} copy(bf16[4,2048,1024]{2,1,0:T(8,128)(2,1)} %all-gather.6.cloned.1.call-done) | data formatting | bytes 33554432
  911.5 0.0 slice-done
  911.5 6.2 copy.63
  (34 shorter events, 0.3 us)
Async XLA Ops:
  7.2 612.0 %all-gather.6.cloned.1.call-start = ((), (), s32[]{:S(2)}) async-start(), calls=%async_computation.5 | async-start | bytes 20971520 | tf_op jit(solution)/shard_map/all_gather | solution.py:47
  15.9 8.7 copy-start.3
  37.8 3.2 collective-permute-start
  38.3 26.6 %collective-permute-start.1 = (bf16[1,256,2048]{1,2,0:T(8,128)(2,1)S(1)}, bf16[1,256,2048]{1,2,0:T(8,128)(2,1)S(1)}, u32[]{:S(2)}, u32[]{:S(2)}) collective-permute-start(bf16[1,256,2048]{1,2,0:T(8,128)(2,1)S(1)} %get-tuple-element.11), channel_id=1, source_target_pairs={{0,2},{1,3},{2,0},{3,1},{4,6},{5,7},{6,4},{7,5},{8,10},{9,11},{10,... | collective-permute-start | bytes 3145736 | tf_op jit(solution)/shard_map/ppermute | solution.py:27
  40.9 46.0 %collective-permute-start.2 = (bf16[1,256,2048]{1,2,0:T(8,128)(2,1)S(1)}, bf16[1,256,2048]{1,2,0:T(8,128)(2,1)S(1)}, u32[]{:S(2)}, u32[]{:S(2)}) collective-permute-start(bf16[1,256,2048]{1,2,0:T(8,128)(2,1)S(1)} %get-tuple-element.10), channel_id=1, source_target_pairs={{0,3},{1,2},{2,1},{3,0},{4,7},{5,6},{6,5},{7,4},{8,11},{9,10},{10,... | collective-permute-start | bytes 3145736 | tf_op jit(solution)/shard_map/ppermute | solution.py:27
  274.6 360.9 %all-gather.8.cloned.1.call-start = ((), (), s32[]{:S(2)}) async-start(), calls=%async_computation.6 | async-start | bytes 20971520 | tf_op jit(solution)/shard_map/all_gather | solution.py:49
  280.7 420.5 %all-gather.4.cloned.1.call-start = ((), (), s32[]{:S(2)}) async-start(), calls=%async_computation.4 | async-start | bytes 20971520 | tf_op jit(solution)/shard_map/all_gather | solution.py:46
  590.4 6.7 copy-start.1
  590.4 16.2 %copy-start = (bf16[768,2048]{1,0:T(8,128)(2,1)S(1)}, bf16[768,2048]{1,0:T(8,128)(2,1)}, u32[]{:S(2)}) copy-start(bf16[768,2048]{1,0:T(8,128)(2,1)} %param.9) | copy-start | bytes 9437188
  597.0 282.1 %reduce-scatter.2.cloned.1.call-start = ((), (), s32[]{:S(2)}) async-start(), calls=%async_computation.7 | async-start | bytes 7077888 | tf_op jit(solution)/shard_map/reduce_scatter | solution.py:83
  610.1 8.9 copy-start.2
  881.1 30.5 %slice-start = ((s8[16777216]{0:T(1024)(128)(4,1)}), s8[4194304]{0:T(1024)(128)(4,1)S(1)}, s32[]{:S(2)}) async-start(s8[16777216]{0:T(1024)(128)(4,1)} %bitcast.62), calls=%async_computation.8 | async-start | bytes 8388608
  881.1 30.5 %slice-start.1 = ((s8[16777216]{0:T(1024)(128)(4,1)}), s8[4194304]{0:T(1024)(128)(4,1)S(1)}, s32[]{:S(2)}) async-start(s8[16777216]{0:T(1024)(128)(4,1)} %bitcast.62), calls=%async_computation.9 | async-start | bytes 8388608
  896.3 15.2 %slice-start.2 = ((s8[16777216]{0:T(1024)(128)(4,1)}), s8[4194304]{0:T(1024)(128)(4,1)S(1)}, s32[]{:S(2)}) async-start(s8[16777216]{0:T(1024)(128)(4,1)} %bitcast.62), calls=%async_computation.10 | async-start | bytes 8388608
  896.3 15.2 %slice-start.3 = ((s8[16777216]{0:T(1024)(128)(4,1)}), s8[4194304]{0:T(1024)(128)(4,1)S(1)}, s32[]{:S(2)}) async-start(s8[16777216]{0:T(1024)(128)(4,1)} %bitcast.62), calls=%async_computation.11 | async-start | bytes 8388608
Sparse Core Ops, SparseCore 0:
  274.7 149.8 all-gather.5
  426.2 104.1 all-gather.7
  597.1 104.0 all-gather.3
  761.1 117.9 reduce-scatter.1
